TPU v7x, 32 devices: a whole 2x2x4 slice. The times are simulated.
32 devices in a mesh: rep: 2 (over x), fs: 8 (over z, y), tp: 2 (over core).
Axes of the slice: x: 2, y: 2, z: 4, core: 2. Of those that a mesh axis runs over, the one named last changes fastest.
Arguments:
- residual: bfloat16 [8192, 2048], P(('rep', 'fs', 'tp')), may hold values from -6 to 6
- mixer_gain: float32 [2048], replicated, may hold values from 0.1 to 1.9
- gating_proj: bfloat16 [2048, 2048], P('fs', 'tp'), may hold values from -0.125 to 0.125
- spatial_proj: bfloat16 [2048, 2048], P('fs', 'tp'), as said below
- spatial_gain: float32 [2048], replicated, may hold values from 0.1 to 1.9
- spatial_bias: float32 [2048], replicated, may hold values from -3 to 3
- spatial_mix: bfloat16 [32, 128, 128], replicated, may hold values from -0.5 to 0.5
- spatial_offset: float32 [32, 128], replicated, may hold values from 0.5 to 1.5
- mixer_out: bfloat16 [2048, 2048], P('tp', 'fs'), may hold values from -0.125 to 0.125
- channel_gain: float32 [2048], replicated, may hold values from 0.1 to 1.9
- gate_proj: bfloat16 [2048, 2816], P('fs', 'tp'), may hold values from -0.125 to 0.125
- up_proj: bfloat16 [2048, 2816], P('fs', 'tp'), may hold values from -0.125 to 0.125
- conv_taps: float32 [3, 2816], replicated, may hold values from -3.5 to 3.5
- down_proj: bfloat16 [2816, 2048], P('tp', 'fs'), may hold values from -0.109375 to 0.109375
Outputs:
- layer_out: bfloat16 [8192, 2048], P(('rep', 'fs', 'tp'))
Inputs may be any that keep to these rules, and one draw needn't show every extreme that they name: `spatial_proj`: entries are bounded in magnitude by 56 / sqrt(2048).
All inputs are finite; a program needn't handle non-finite values.
Results may differ from a plain program's by a relative error of at most 0.015.
Values may be sent and summed in bfloat16 or wider, within the bound.
A program may use at most 128 MiB of HBM per device.

v0:
```python
import functools

import jax
import jax.numpy as jnp
from jax import lax
from jax.experimental import pallas as pl
from jax.experimental.pallas import tpu as pltpu
from jax.sharding import PartitionSpec as P

HEAD = 64
SEGMENT = 64
KCONV = 3
SEQ_LEN = 256
LANES = 128

MESH = pl.DeviceIdType.MESH
BF16, F32 = jnp.bfloat16, jnp.float32

PHASES = ((0, 1), (2,), (3, 4), (5,))
STREAMS = 6


def dot(a, b):
    return jnp.dot(a, b, preferred_element_type=F32)


def kernel(
    dims,
    residual,
    gating,
    spatial,
    mixer_out,
    gate,
    up,
    down,
    mix,
    mixer_gain,
    channel_gain,
    spatial_gain,
    spatial_bias,
    offset,
    taps,
    out,
    g0,
    g1,
    g2,
    g3,
    g4,
    g5,
    rows_in,
    normed,
    middle,
    act_u,
    act_v,
    gated,
    hidden,
    mixw,
    wcat,
    offs,
    stat,
    part_out,
    part_in,
    sum_out,
    sum_in,
    part_out2,
    part_in2,
    sum_out2,
    sum_in2,
    local_sem,
    recv_sem,
    own_sem,
    z_sem,
    y_sem,
    row_send,
    row_recv,
    stat_send,
    stat_recv,
    part_send,
    part_recv,
    sum_send,
    sum_recv,
    mid_send,
    mid_recv,
    part_send2,
    part_recv2,
    sum_send2,
    sum_recv2,
):
    fs, rows, depth, group, width, units = dims
    lines = fs // 2
    blocks = (g0, g1, g2, g3, g4, g5)
    r, f, c = lax.axis_index("rep"), lax.axis_index("fs"), lax.axis_index("tp")
    q, y = f // 2, f % 2
    mine = c * 2 + r
    beside = c * 2 + 1 - r
    peers = (1 - c) * 2
    left, right = (r, f - 2, c), (r, f + 2, c)
    across, pair = (r, f + 1 - 2 * y, c), (1 - r, f, c)
    twin, diag = (r, f, 1 - c), (1 - r, f, 1 - c)
    has_left, has_right = q > 0, q < lines - 1

    def remote(src, dst, send, recv, device):
        return pltpu.make_async_remote_copy(
            src_ref=src,
            dst_ref=dst,
            send_sem=send,
            recv_sem=recv,
            device_id=device,
            device_id_type=MESH,
        )

    own = (
        gating.at[:, pl.ds(pl.multiple_of(r * width, LANES), width)],
        spatial.at[:, pl.ds(pl.multiple_of(r * width, LANES), width)],
        mixer_out.at[pl.ds(pl.multiple_of(r * width, 16), width)],
        gate,
        up,
        down.at[pl.ds(pl.multiple_of(r * units, 16), units)],
    )
    heads = mixw.shape[0]
    head = mine * heads
    own_copies = [
        pltpu.make_async_copy(own[s], blocks[s].at[f], local_sem.at[s]) for s in range(STREAMS)
    ]
    row_copy = pltpu.make_async_copy(residual, rows_in.at[mine], local_sem.at[STREAMS])
    mix_copy = pltpu.make_async_copy(mix.at[pl.ds(head, heads)], mixw, local_sem.at[STREAMS + 1])
    for copy in own_copies[:2] + [row_copy] + own_copies[2:] + [mix_copy]:
        copy.start()

    barrier = pltpu.get_barrier_semaphore()
    for device in (across, pair, twin, diag):
        pl.semaphore_signal(barrier, inc=1, device_id=device, device_id_type=MESH)

    @pl.when(has_left)
    def _():
        pl.semaphore_signal(barrier, inc=1, device_id=left, device_id_type=MESH)

    @pl.when(has_right)
    def _():
        pl.semaphore_signal(barrier, inc=1, device_id=right, device_id_type=MESH)

    pl.semaphore_wait(barrier, 4 + jnp.minimum(q, 1) + jnp.minimum(lines - 1 - q, 1))

    def block(s, source, send, device):
        ref = blocks[s].at[source]
        return remote(ref, ref, send, recv_sem.at[s, source], device)

    def arrived(s, source):
        block(s, source, y_sem.at[s, source], across).wait_recv()

    def send_own(s):
        own_copies[s].wait()

        @pl.when(has_left)
        def _():
            block(s, f, own_sem.at[s], left).start()

        @pl.when(has_right)
        def _():
            block(s, f, z_sem.at[s, f], right).start()

        block(s, f, y_sem.at[s, f], across).start()

    def step(s, d):
        @pl.when(q - d >= 0)
        def _():
            source = f - 2 * d
            arrived(s, source)

            @pl.when(has_right)
            def _():
                block(s, source, z_sem.at[s, source], right).start()

            block(s, source, y_sem.at[s, source], across).start()

        @pl.when(q + d < lines)
        def _():
            source = f + 2 * d
            arrived(s, source)

            @pl.when(has_left)
            def _():
                block(s, source, z_sem.at[s, source], left).start()

            block(s, source, y_sem.at[s, source], across).start()

    def steps(p, d):
        for s in PHASES[p]:
            step(s, d)

    def crossed(p):
        for s in PHASES[p]:

            @pl.loop(0, lines)
            def _(k):
                arrived(s, 2 * k + 1 - y)

    for s in PHASES[0]:
        send_own(s)
    row_to_pair = remote(
        residual, rows_in.at[mine], row_send.at[0], row_recv.at[mine], pair
    )
    row_to_twin = remote(
        residual, rows_in.at[mine], row_send.at[1], row_recv.at[mine], twin
    )
    row_to_pair.start()
    row_to_twin.start()
    for s in PHASES[1]:
        send_own(s)

    def row_wait(slot):
        remote(
            rows_in.at[slot], rows_in.at[slot], row_send.at[0], row_recv.at[slot], pair
        ).wait_recv()

    tile = 64

    def norm_in(slot):
        @pl.loop(0, rows // tile)
        def _(i):
            here = pl.ds(pl.multiple_of(i * tile, tile), tile)
            wide = rows_in[slot, here, :].astype(F32)
            scale = lax.rsqrt(jnp.mean(wide * wide, axis=-1, keepdims=True) + 1e-06)
            normed[slot, here, :] = (wide * scale * mixer_gain[...]).astype(BF16)

    row_copy.wait()
    norm_in(mine)
    steps(0, 1)
    for s in PHASES[2]:
        send_own(s)
    row_wait(beside)
    row_forward = remote(
        rows_in.at[beside], rows_in.at[beside], row_send.at[2], row_recv.at[beside], twin
    )
    row_forward.start()
    norm_in(beside)
    for j in range(2):
        row_wait(peers + j)
        norm_in(peers + j)

    mix_copy.wait()
    span = mixw.shape[1]
    per = LANES // HEAD
    at_row = lax.broadcasted_iota(jnp.int32, (span, span), 0)
    at_col = lax.broadcasted_iota(jnp.int32, (span, span), 1)
    allowed = at_col // SEGMENT <= at_row // SEGMENT
    eye = at_col == at_row
    lane = lax.broadcasted_iota(jnp.int32, (span, LANES), 1)

    def column_of(row):
        return jnp.sum(
            jnp.where(eye, jnp.broadcast_to(row, (span, span)), 0.0), axis=1, keepdims=True
        )

    def row_of(column):
        return jnp.sum(
            jnp.where(eye, jnp.broadcast_to(column, (span, span)), 0.0), axis=0, keepdims=True
        )

    for p in range(heads // per):
        off = jnp.zeros((span, LANES), F32)
        for k in range(per):
            h = p * per + k
            wcat[p, :, k * span : (k + 1) * span] = jnp.where(
                allowed, mixw[h].astype(F32), 0.0
            ).astype(BF16)
            here = column_of(offset[pl.ds(head + h, 1), :])
            off = jnp.where(lane // HEAD == k, here, off)
        offs[:, p * LANES : (p + 1) * LANES] = off

    for d in range(2, lines):
        steps(0, d)
    crossed(0)

    def project(slot):
        n = normed[slot]
        u = dot(n, g0[...].reshape(depth, width)).astype(BF16).astype(F32)
        act_u[slot] = jax.nn.gelu(u)
        v = jax.nn.gelu(dot(n, g1[...].reshape(depth, width)).astype(BF16).astype(F32))
        act_v[slot] = v
        total = jnp.sum(v, axis=-1, keepdims=True)
        squares = jnp.sum(v * v, axis=-1, keepdims=True)
        for b in range(rows // span):
            here = pl.ds(pl.multiple_of(slot * rows + b * span, LANES), span)
            stat[mine, 0:1, here] = row_of(total[b * span : (b + 1) * span])
            stat[mine, 1:2, here] = row_of(squares[b * span : (b + 1) * span])

    @pl.loop(0, 4)
    def _(slot):
        project(slot)
        for s in PHASES[1]:

            @pl.when(slot + 1 < lines)
            def _():
                step(s, slot + 1)

    for s in PHASES[1]:
        for d in range(5, lines):
            step(s, d)

    stat_copies = [
        remote(stat.at[mine], stat.at[mine], stat_send.at[i], stat_recv.at[mine], device)
        for i, device in enumerate((pair, twin, diag))
    ]
    for copy in stat_copies:
        copy.start()
    for s in PHASES[3]:
        send_own(s)
    for other in (beside, peers, peers + 1):
        remote(
            stat.at[other], stat.at[other], stat_send.at[0], stat_recv.at[other], pair
        ).wait_recv()

    gain_here = spatial_gain[:, pl.ds(pl.multiple_of(mine * width, LANES), width)]
    bias_here = spatial_bias[:, pl.ds(pl.multiple_of(mine * width, LANES), width)]
    pairs = heads // per

    def gate_slot(slot):
        low, high = [], []
        for b in range(rows // span):
            here = pl.ds(pl.multiple_of(slot * rows + b * span, LANES), span)
            sums = stat[0, :, here] + stat[1, :, here] + stat[2, :, here] + stat[3, :, here]
            mean_row = sums[0:1] / group
            var_row = sums[1:2] / group - mean_row * mean_row
            mean = column_of(mean_row)
            scale = lax.rsqrt(column_of(var_row) + 1e-05)
            v = act_v[slot, b * span : (b + 1) * span, :]
            vnorm = (v - mean) * scale * gain_here + bias_here
            parts = []
            for p in range(pairs):
                tile_v = vnorm[:, p * LANES : (p + 1) * LANES]
                parts.append(
                    jnp.concatenate(
                        [
                            jnp.where(lane // HEAD == k, tile_v, 0.0).astype(BF16)
                            for k in range(per)
                        ],
                        axis=0,
                    )
                )
            low.append(parts)
        for p in range(pairs):
            rhs = jnp.concatenate([parts[p] for parts in low], axis=1)
            mixed = dot(wcat[p], rhs)
            here = slice(p * LANES, (p + 1) * LANES)
            for b in range(rows // span):
                there = slice(b * span, (b + 1) * span)
                m = mixed[:, b * LANES : (b + 1) * LANES] + offs[:, here]
                gated[slot, there, here] = (act_u[slot, there, here] * m).astype(BF16)

    @pl.loop(0, 4)
    def _(slot):
        gate_slot(slot)

    crossed(1)

    model = g2.shape[2]

    def product(lhs, weights, k):
        return [dot(lhs, weights[2 * k + j]) for j in range(2)]

    def copy_of(src, dst, send, recv, k, j, device):
        return remote(src.at[k, j], dst.at[k, j], send.at[k, j], recv.at[k, j], device)

    @pl.loop(0, lines)
    def _(k):
        for j in range(2):
            for i, value in enumerate(product(gated[peers + j], g2, k)):
                part_out[k, j, :, i * model : (i + 1) * model] = value.astype(BF16)
            copy_of(part_out, part_in, part_send, part_recv, k, j, twin).start()

    @pl.loop(0, lines)
    def _(k):
        for j in range(2):
            values = product(gated[c * 2 + j], g2, k)
            copy_of(part_out, part_in, part_send, part_recv, k, j, twin).wait_recv()
            for i, value in enumerate(values):
                here = slice(i * model, (i + 1) * model)
                sum_out[k, j, :, here] = (value + part_in[k, j, :, here].astype(F32)).astype(BF16)
            copy_of(sum_out, sum_in, sum_send, sum_recv, k, j, pair).start()

    def mid_copy(k, slot):
        return remote(
            middle.at[k, slot], middle.at[k, slot], mid_send.at[k, slot], mid_recv.at[k, slot], twin
        )

    @pl.loop(0, lines)
    def _(k):
        for j in range(2):
            copy_of(sum_out, sum_in, sum_send, sum_recv, k, j, pair).wait_recv()
            here = pl.ds(pl.multiple_of(k * 2 * model, LANES), 2 * model)
            slot = c * 2 + j
            total = sum_out[k, j].astype(F32) + sum_in[k, j].astype(F32)
            middle[k, slot] = (rows_in[slot, :, here].astype(F32) + total).astype(BF16)
            mid_copy(k, slot).start()

        for s in PHASES[2]:

            @pl.when(k + 1 < lines)
            def _():
                step(s, k + 1)

    def norm_middle(slot):
        @pl.loop(0, rows // tile)
        def _(i):
            here = pl.ds(pl.multiple_of(i * tile, tile), tile)
            wide = [middle[k, slot, here, :].astype(F32) for k in range(lines)]
            total = sum(jnp.sum(w * w, axis=-1, keepdims=True) for w in wide)
            scale = lax.rsqrt(total / depth + 1e-06)
            for k in range(lines):
                there = slice(k * 2 * model, (k + 1) * 2 * model)
                normed[slot, here, there] = (wide[k] * scale * channel_gain[:, there]).astype(BF16)

    for j in range(2):
        norm_middle(c * 2 + j)
    for j in range(2):

        @pl.loop(0, lines)
        def _(k):
            mid_copy(k, peers + j).wait_recv()

        norm_middle(peers + j)

    steps(3, 1)
    crossed(2)

    place = lax.broadcasted_iota(jnp.int32, (rows, units), 0) % SEQ_LEN

    def channel(slot):
        n = normed[slot]
        gates = dot(n, g3[...].reshape(depth, units)).astype(BF16).astype(F32)
        conv = taps[KCONV - 1 : KCONV, :] * gates
        for lag in range(1, KCONV):
            shifted = jnp.where(place >= lag, pltpu.roll(gates, lag, 0), 0.0)
            conv = conv + taps[KCONV - 1 - lag : KCONV - lag, :] * shifted
        ups = dot(n, g4[...].reshape(depth, units)).astype(BF16).astype(F32)
        hidden[slot] = (jax.nn.silu(conv) * ups).astype(BF16)

    @pl.loop(0, 4)
    def _(slot):
        channel(slot)

        @pl.when(slot + 2 < lines)
        def _():
            for s in PHASES[3]:
                step(s, slot + 2)

    for s in PHASES[3]:
        for d in range(6, lines):
            step(s, d)
    crossed(3)

    @pl.loop(0, lines)
    def _(k):
        for j in range(2):
            for i, value in enumerate(product(hidden[peers + j], g5, k)):
                part_out2[k, j, :, i * model : (i + 1) * model] = value.astype(BF16)
            copy_of(part_out2, part_in2, part_send2, part_recv2, k, j, twin).start()

    def sum_copy(k):
        return remote(
            sum_out2.at[k], sum_in2.at[k], sum_send2.at[k], sum_recv2.at[k], pair
        )

    @pl.loop(0, lines)
    def _(k):
        values = product(hidden[beside], g5, k)
        copy_of(part_out2, part_in2, part_send2, part_recv2, k, 1 - r, twin).wait_recv()
        for i, value in enumerate(values):
            here = slice(i * model, (i + 1) * model)
            sum_out2[k, :, here] = (value + part_in2[k, 1 - r, :, here].astype(F32)).astype(BF16)
        sum_copy(k).start()

    @pl.loop(0, lines)
    def _(k):
        values = product(hidden[mine], g5, k)
        copy_of(part_out2, part_in2, part_send2, part_recv2, k, r, twin).wait_recv()
        sum_copy(k).wait_recv()
        for i, value in enumerate(values):
            here = slice(i * model, (i + 1) * model)
            total = value + part_in2[k, r, :, here].astype(F32)
            total = total + sum_in2[k, :, here].astype(F32)
            total = total + middle[k, mine, :, here].astype(F32)
            act = total.astype(BF16)
            for kk in range(lines):

                @pl.when(k == kk)
                def _():
                    at = (2 * kk + i) * model
                    out[:, at : at + model] = act

    for s in range(STREAMS):

        @pl.when(has_left)
        def _():
            block(s, f, own_sem.at[s], left).wait_send()

        @pl.loop(0, lines)
        def _(k):
            source = 2 * k + y
            block(s, source, y_sem.at[s, source], across).wait_send()

            @pl.when(((k <= q) & has_right) | ((k > q) & has_left))
            def _():
                block(s, source, z_sem.at[s, source], across).wait_send()

    for copy in (row_to_pair, row_to_twin, row_forward, *stat_copies):
        copy.wait_send()

    @pl.loop(0, lines)
    def _(k):
        for j in range(2):
            copy_of(part_out, part_in, part_send, part_recv, k, j, twin).wait_send()
            copy_of(sum_out, sum_in, sum_send, sum_recv, k, j, pair).wait_send()
            copy_of(part_out2, part_in2, part_send2, part_recv2, k, j, twin).wait_send()
            mid_copy(k, c * 2 + j).wait_send()
        sum_copy(k).wait_send()


def body(reps, fs, tps):
    assert reps == 2 and tps == 2 and fs % 2 == 0

    def on_device(
        residual,
        mixer_gain,
        gating_proj,
        spatial_proj,
        spatial_gain,
        spatial_bias,
        spatial_mix,
        spatial_offset,
        mixer_out,
        channel_gain,
        gate_proj,
        up_proj,
        conv_taps,
        down_proj,
    ):
        r, c = lax.axis_index("rep"), lax.axis_index("tp")
        rows, depth = residual.shape
        assert rows % SEQ_LEN == 0
        own_rows = gating_proj.shape[0]
        width = gating_proj.shape[1] // reps
        units = gate_proj.shape[1] // reps
        group = gating_proj.shape[1] * tps
        columns = mixer_out.shape[1]
        span = spatial_mix.shape[1]
        heads = width // HEAD
        lines = fs // 2
        gate_here = lax.dynamic_slice_in_dim(gate_proj, r * units, units, 1)
        up_here = lax.dynamic_slice_in_dim(up_proj, r * units, units, 1)
        taps_here = lax.dynamic_slice_in_dim(conv_taps, (c * reps + r) * units, units, 1)
        vmem, hbm = pl.BlockSpec(memory_space=pltpu.VMEM), pl.BlockSpec(memory_space=pl.ANY)
        dma = pltpu.SemaphoreType.DMA
        wide = 2 * columns
        return pl.pallas_call(
            functools.partial(kernel, (fs, rows, depth, group, width, units)),
            out_shape=jax.ShapeDtypeStruct((rows, depth), BF16),
            in_specs=[hbm] * 8 + [vmem] * 6,
            out_specs=vmem,
            scratch_shapes=[
                pltpu.VMEM((fs, own_rows, width), BF16),
                pltpu.VMEM((fs, own_rows, width), BF16),
                pltpu.VMEM((fs, width, columns), BF16),
                pltpu.VMEM((fs, own_rows, units), BF16),
                pltpu.VMEM((fs, own_rows, units), BF16),
                pltpu.VMEM((fs, units, columns), BF16),
                pltpu.VMEM((4, rows, depth), BF16),
                pltpu.VMEM((4, rows, depth), BF16),
                pltpu.VMEM((lines, 4, rows, wide), BF16),
                pltpu.VMEM((4, rows, width), F32),
                pltpu.VMEM((4, rows, width), F32),
                pltpu.VMEM((4, rows, width), BF16),
                pltpu.VMEM((4, rows, units), BF16),
                pltpu.VMEM((heads, span, span), BF16),
                pltpu.VMEM((heads * HEAD // LANES, span, span * LANES // HEAD), BF16),
                pltpu.VMEM((span, width), F32),
                pltpu.VMEM((4, 2, 4 * rows), F32),
                pltpu.VMEM((lines, 2, rows, wide), BF16),
                pltpu.VMEM((lines, 2, rows, wide), BF16),
                pltpu.VMEM((lines, 2, rows, wide), BF16),
                pltpu.VMEM((lines, 2, rows, wide), BF16),
                pltpu.VMEM((lines, 2, rows, wide), BF16),
                pltpu.VMEM((lines, 2, rows, wide), BF16),
                pltpu.VMEM((lines, rows, wide), BF16),
                pltpu.VMEM((lines, rows, wide), BF16),
                dma((STREAMS + 2,)),
                dma((STREAMS, fs)),
                dma((STREAMS,)),
                dma((STREAMS, fs)),
                dma((STREAMS, fs)),
                dma((3,)),
                dma((4,)),
                dma((3,)),
                dma((4,)),
                dma((lines, 2)),
                dma((lines, 2)),
                dma((lines, 2)),
                dma((lines, 2)),
                dma((lines, 4)),
                dma((lines, 4)),
                dma((lines, 2)),
                dma((lines, 2)),
                dma((lines,)),
                dma((lines,)),
            ],
            compiler_params=pltpu.CompilerParams(
                collective_id=0, has_side_effects=True, vmem_limit_bytes=67043328
            ),
        )(
            residual,
            gating_proj,
            spatial_proj,
            mixer_out,
            gate_here,
            up_here,
            down_proj,
            spatial_mix,
            mixer_gain.reshape(1, -1),
            channel_gain.reshape(1, -1),
            spatial_gain.reshape(1, -1),
            spatial_bias.reshape(1, -1),
            spatial_offset,
            taps_here,
        )

    return on_device


def solution(mesh):
    in_specs = (
        P(("rep", "fs", "tp"), None),
        P(),
        P("fs", "tp"),
        P("fs", "tp"),
        P(),
        P(),
        P(),
        P(),
        P("tp", "fs"),
        P(),
        P("fs", "tp"),
        P("fs", "tp"),
        P(),
        P("tp", "fs"),
    )
    out_specs = P(("rep", "fs", "tp"), None)
    return jax.shard_map(
        body(mesh.shape["rep"], mesh.shape["fs"], mesh.shape["tp"]),
        mesh=mesh,
        in_specs=in_specs,
        out_specs=out_specs,
        check_vma=False,
    )
```

profile of v0, /device:TPU:0, one launch (start us, length us, event | category | flops | bytes accessed | tf_op | source)
XLA Modules:
  0.0 226.1 jit_solution(4983360794179790468)
XLA Ops:
  0.0 1.4 constant_dynamic-slice_fusion.taps
  1.4 2.5 %constant_dynamic-slice_fusion.1 = (bf16[256,704]{1,0:T(8,128)(2,1)}, bf16[256,704]{1,0:T(8,128)(2,1)}) fusion(bf16[256,1408]{1,0:T(8,128)(2,1)} %param.25, s32[]{:T(128)S(6)} %select_n.7, bf16[256,1408]{1,0:T(8,128)(2,1)} %param.24), kind=kLoop, calls=%fused_computation.1 | loop fusion | bytes 1441796 | tf_op jit(solution)/shard_map/dynamic_slice | solution.py:551
  3.9 219.9 %shard_map.136 = bf16[256,2048]{1,0:T(8,128)(2,1)} custom-call(bf16[256,2048]{1,0:T(8,128)(2,1)} %residual.1, bf16[256,1024]{1,0:T(8,128)(2,1)} %gating.1, bf16[256,1024]{1,0:T(8,128)(2,1)} %spatial.1, bf16[1024,256]{1,0:T(8,128)(2,1)} %mixer_out.1, bf16[256,704]{1,0:T(8,128)(2,1)} %get-tuple-element.6.gate, bf16[256,704]{1,0:T(8,128)(2,1)} %get-tuple-element.5.up, ...), custom_call_target="tpu_custom_call" | custom-call | tf_op jit(solution)/shard_map/pallas_call | solution.py:556
  223.8 2.3 %copy.16 = bf16[256,2048]{1,0:T(8,128)(2,1)} copy(bf16[256,2048]{1,0:T(8,128)(2,1)} %shard_map.136) | data formatting | bytes 2097152
where the time goes:
time: 226 us
  Pallas kernels  220 us (97%)
  local copies, waits for them, and re-layouts  6.18 us (3%)
    pallas_call x1, Pallas kernels, on_device(): pl.pallas_call(functools.partial(kernel, (fs, rows, depth, group, width,...  220 us

commit v1 on v0

v1 whole, which is shorter than its diff:
```python
import functools

import jax
import jax.numpy as jnp
from jax import lax
from jax.experimental import pallas as pl
from jax.experimental.pallas import tpu as pltpu
from jax.sharding import PartitionSpec as P

HEAD = 64
SEGMENT = 64
KCONV = 3
SEQ_LEN = 256
LANES = 128

MESH = pl.DeviceIdType.MESH
BF16, F32 = jnp.bfloat16, jnp.float32

PHASES = ((0, 1), (2,), (3, 4), (5,))
STREAMS = 6
BY_COPY = (3, 4)


def dot(a, b):
    return jnp.dot(a, b, preferred_element_type=F32)


def kernel(
    dims,
    residual,
    gating,
    spatial,
    mixer_out,
    gate,
    up,
    down,
    mix,
    mixer_gain,
    channel_gain,
    spatial_gain,
    spatial_bias,
    offset,
    taps,
    out,
    g0,
    g1,
    g2,
    g3,
    g4,
    g5,
    raw,
    cross,
    taps_here,
    rows_in,
    normed,
    middle,
    act_u,
    act_v,
    gated,
    hidden,
    mixw,
    wcat,
    offs,
    stat,
    part_out,
    part_in,
    sum_out,
    sum_in,
    last_in,
    local_sem,
    line_recv,
    pair_recv,
    left_send,
    line_send,
    pair_send,
    cross_send,
    row_send,
    row_recv,
    stat_send,
    stat_recv,
    part_send,
    part_recv,
    sum_send,
    sum_recv,
    mid_send,
    mid_recv,
    part_send2,
    part_recv2,
    last_send,
    last_recv,
):
    fs, rows, depth, group, width, units = dims
    lines = fs // 2
    blocks = (g0, g1, g2, g3, g4, g5)
    halves = [block.shape[1] // 2 for block in blocks]
    r, f, c = lax.axis_index("rep"), lax.axis_index("fs"), lax.axis_index("tp")
    q, y = f // 2, f % 2
    beyond = f + 1 - 2 * y
    mine = c * 2 + y
    beside = c * 2 + 1 - y
    peers = (1 - c) * 2
    left, right = (r, f - 2, c), (r, f + 2, c)
    across, copy_chip = (r, beyond, c), (1 - r, f, c)
    twin, diag = (r, f, 1 - c), (r, beyond, 1 - c)
    has_left, has_right = q > 0, q < lines - 1

    def remote(src, dst, send, recv, device):
        return pltpu.make_async_remote_copy(
            src_ref=src,
            dst_ref=dst,
            send_sem=send,
            recv_sem=recv,
            device_id=device,
            device_id_type=MESH,
        )

    def at(start, size, step):
        return pl.ds(pl.multiple_of(start, step), size)

    own_copies = {
        0: (gating.at[:, at(y * width, width, LANES)], g0.at[f]),
        1: (spatial.at[:, at(y * width, width, LANES)], g1.at[f]),
        2: (mixer_out.at[at(y * width, width, 16)], g2.at[f]),
        3: (gate, raw.at[0]),
        4: (up, raw.at[1]),
        5: (down.at[at(y * units, units, 16)], g5.at[f]),
    }
    own_copies = [
        pltpu.make_async_copy(*own_copies[s], local_sem.at[s]) for s in range(STREAMS)
    ]
    heads = mixw.shape[0]
    head = mine * heads
    row_copy = pltpu.make_async_copy(residual, rows_in.at[mine], local_sem.at[STREAMS])
    mix_copy = pltpu.make_async_copy(mix.at[pl.ds(head, heads)], mixw, local_sem.at[STREAMS + 1])
    for copy in own_copies[:2] + [row_copy] + own_copies[2:] + [mix_copy]:
        copy.start()

    barrier = pltpu.get_barrier_semaphore()
    for device in (across, copy_chip, twin, diag):
        pl.semaphore_signal(barrier, inc=1, device_id=device, device_id_type=MESH)

    @pl.when(has_left)
    def _():
        pl.semaphore_signal(barrier, inc=1, device_id=left, device_id_type=MESH)

    @pl.when(has_right)
    def _():
        pl.semaphore_signal(barrier, inc=1, device_id=right, device_id_type=MESH)

    pl.semaphore_wait(barrier, 4 + jnp.minimum(q, 1) + jnp.minimum(lines - 1 - q, 1))

    def half(s, source, h):
        return blocks[s].at[source, at(h * halves[s], halves[s], 16)]

    def on_line(s, source, send, device):
        ref = half(s, source, r)
        return remote(ref, ref, send, line_recv.at[s, source], device)

    def to_copy(s, source):
        ref = half(s, source, r)
        return remote(ref, ref, pair_send.at[s, source], pair_recv.at[s, source], copy_chip)

    def line_wait(s, source):
        on_line(s, source, line_send.at[s, source], across).wait_recv()

    def pair_wait(s, source):
        ref = half(s, source, 1 - r)
        remote(
            ref, ref, pair_send.at[s, source], pair_recv.at[s, source], copy_chip
        ).wait_recv()

    def crossing(s, h):
        start = (1 - y) * width
        here = at(h * halves[s], halves[s], 16)
        if s < 2:
            src = (gating, spatial)[s].at[here, at(start, width, LANES)]
        elif s == 2:
            src = mixer_out.at[at(start + h * halves[s], halves[s], 16)]
        elif s < 5:
            src = cross.at[s - 3, here]
        else:
            src = down.at[at((1 - y) * units + h * halves[s], halves[s], 16)]
        return src, half(s, f, h)

    def cross_line(s):
        src, dst = crossing(s, r)
        return remote(src, dst, cross_send.at[s, 0], line_recv.at[s, f], across)

    def cross_pair(s):
        src, dst = crossing(s, 1 - r)
        return remote(src, dst, cross_send.at[s, 1], pair_recv.at[s, f], across)

    def both_ways(s, source):
        @pl.when(has_left)
        def _():
            on_line(s, source, left_send.at[s, source % 2], left).start()

        @pl.when(has_right)
        def _():
            on_line(s, source, line_send.at[s, source], right).start()

    def own(p):
        for s in PHASES[p]:
            both_ways(s, f)

    def crossed(p):
        for s in PHASES[p]:
            line_wait(s, beyond)
            both_ways(s, beyond)
            if s in BY_COPY:
                to_copy(s, beyond).start()

    def step(s, d, other):
        @pl.when(q - d >= 0)
        def _():
            source = (beyond if other else f) - 2 * d
            line_wait(s, source)

            @pl.when(has_right)
            def _():
                on_line(s, source, line_send.at[s, source], right).start()

            to_copy(s, source).start()

        @pl.when(q + d < lines)
        def _():
            source = (beyond if other else f) + 2 * d
            line_wait(s, source)

            @pl.when(has_left)
            def _():
                on_line(s, source, line_send.at[s, source], left).start()

            to_copy(s, source).start()

    def steps(p, d):
        for other in (False, True):
            for s in PHASES[p]:
                step(s, d, other)

    def complete(s):
        @pl.loop(0, fs)
        def _(source):
            @pl.when(source != f)
            def _():
                pair_wait(s, source)

    row_to_across = remote(residual, rows_in.at[mine], row_send.at[0], row_recv.at[mine], across)
    row_to_twin = remote(residual, rows_in.at[mine], row_send.at[1], row_recv.at[mine], twin)
    for s in PHASES[0] + PHASES[1]:
        cross_line(s).start()
    row_to_across.start()
    row_to_twin.start()
    for s in PHASES[0]:
        cross_pair(s).start()
    for p in range(2):
        for s in PHASES[p]:
            own_copies[s].wait()
        own(p)

    def row_wait(slot):
        remote(
            rows_in.at[slot], rows_in.at[slot], row_send.at[0], row_recv.at[slot], across
        ).wait_recv()

    tile = 64

    def norm_in(slot):
        @pl.loop(0, rows // tile)
        def _(i):
            here = pl.ds(pl.multiple_of(i * tile, tile), tile)
            wide = rows_in[slot, here, :].astype(F32)
            scale = lax.rsqrt(jnp.mean(wide * wide, axis=-1, keepdims=True) + 1e-06)
            normed[slot, here, :] = (wide * scale * mixer_gain[...]).astype(BF16)

    for i, s in enumerate(PHASES[2]):
        own_copies[s].wait()
        for way in range(2):

            @pl.when(y == way)
            def _():
                blocks[s][f] = raw[i, :, way * units : (way + 1) * units]
                cross[i] = raw[i, :, (1 - way) * units : (2 - way) * units]

    for k in range(4):

        @pl.when(mine == k)
        def _():
            taps_here[...] = taps[:, k * units : (k + 1) * units]

    for s in PHASES[2] + PHASES[1] + PHASES[3]:
        if s in PHASES[1]:
            cross_pair(s).start()
        else:
            cross_line(s).start()
    row_copy.wait()
    norm_in(mine)
    own_copies[5].wait()
    mix_copy.wait()

    crossed(0)
    for d in range(1, lines - 1):
        steps(0, d)
    row_wait(beside)
    row_forward = remote(
        rows_in.at[beside], rows_in.at[beside], row_send.at[2], row_recv.at[beside], twin
    )
    row_forward.start()
    norm_in(beside)
    steps(0, lines - 1)
    crossed(1)
    own(2)
    for j in range(2):
        row_wait(peers + j)
        norm_in(peers + j)

    span = mixw.shape[1]
    per = LANES // HEAD
    at_row = lax.broadcasted_iota(jnp.int32, (span, span), 0)
    at_col = lax.broadcasted_iota(jnp.int32, (span, span), 1)
    allowed = at_col // SEGMENT <= at_row // SEGMENT
    eye = at_col == at_row
    lane = lax.broadcasted_iota(jnp.int32, (span, LANES), 1)

    def column_of(row):
        return jnp.sum(
            jnp.where(eye, jnp.broadcast_to(row, (span, span)), 0.0), axis=1, keepdims=True
        )

    def row_of(column):
        return jnp.sum(
            jnp.where(eye, jnp.broadcast_to(column, (span, span)), 0.0), axis=0, keepdims=True
        )

    for p in range(heads // per):
        off = jnp.zeros((span, LANES), F32)
        for k in range(per):
            h = p * per + k
            wcat[p, :, k * span : (k + 1) * span] = jnp.where(
                allowed, mixw[h].astype(F32), 0.0
            ).astype(BF16)
            here = column_of(offset[pl.ds(head + h, 1), :])
            off = jnp.where(lane // HEAD == k, here, off)
        offs[:, p * LANES : (p + 1) * LANES] = off

    for s in PHASES[0]:
        complete(s)

    def project(slot):
        n = normed[slot]
        u = dot(n, g0[...].reshape(depth, width)).astype(BF16).astype(F32)
        act_u[slot] = jax.nn.gelu(u)
        v = jax.nn.gelu(dot(n, g1[...].reshape(depth, width)).astype(BF16).astype(F32))
        act_v[slot] = v
        total = jnp.sum(v, axis=-1, keepdims=True)
        squares = jnp.sum(v * v, axis=-1, keepdims=True)
        for b in range(rows // span):
            here = pl.ds(pl.multiple_of(slot * rows + b * span, LANES), span)
            stat[mine, 0:1, here] = row_of(total[b * span : (b + 1) * span])
            stat[mine, 1:2, here] = row_of(squares[b * span : (b + 1) * span])

    @pl.loop(0, 4)
    def _(slot):
        project(slot)

        @pl.when(slot + 1 < lines)
        def _():
            steps(1, slot + 1)

    for d in range(5, lines):
        steps(1, d)

    stat_copies = [
        remote(stat.at[mine], stat.at[mine], stat_send.at[i], stat_recv.at[mine], device)
        for i, device in enumerate((across, twin, diag))
    ]
    for copy in stat_copies:
        copy.start()
    crossed(2)
    own(3)
    for other in (beside, peers, peers + 1):
        remote(
            stat.at[other], stat.at[other], stat_send.at[0], stat_recv.at[other], across
        ).wait_recv()

    gain_here = spatial_gain[:, pl.ds(pl.multiple_of(mine * width, LANES), width)]
    bias_here = spatial_bias[:, pl.ds(pl.multiple_of(mine * width, LANES), width)]
    pairs = heads // per

    def gate_slot(slot):
        low = []
        for b in range(rows // span):
            here = pl.ds(pl.multiple_of(slot * rows + b * span, LANES), span)
            sums = stat[0, :, here] + stat[1, :, here] + stat[2, :, here] + stat[3, :, here]
            mean_row = sums[0:1] / group
            var_row = sums[1:2] / group - mean_row * mean_row
            mean = column_of(mean_row)
            scale = lax.rsqrt(column_of(var_row) + 1e-05)
            v = act_v[slot, b * span : (b + 1) * span, :]
            vnorm = (v - mean) * scale * gain_here + bias_here
            parts = []
            for p in range(pairs):
                tile_v = vnorm[:, p * LANES : (p + 1) * LANES]
                parts.append(
                    jnp.concatenate(
                        [
                            jnp.where(lane // HEAD == k, tile_v, 0.0).astype(BF16)
                            for k in range(per)
                        ],
                        axis=0,
                    )
                )
            low.append(parts)
        for p in range(pairs):
            rhs = jnp.concatenate([parts[p] for parts in low], axis=1)
            mixed = dot(wcat[p], rhs)
            here = slice(p * LANES, (p + 1) * LANES)
            for b in range(rows // span):
                there = slice(b * span, (b + 1) * span)
                m = mixed[:, b * LANES : (b + 1) * LANES] + offs[:, here]
                gated[slot, there, here] = (act_u[slot, there, here] * m).astype(BF16)

    @pl.loop(0, 4)
    def _(slot):
        gate_slot(slot)

    model = g2.shape[2]
    near = jnp.minimum(q, lines - 1 - q)

    def nth(i):
        d = (i + 1) // 2
        close = jnp.where(i % 2 == 1, q + d, q - d)
        far = jnp.where(q < lines - 1 - q, i, lines - 1 - i)
        return jnp.where(i <= 2 * near, close, far)

    def of_unit(i):
        k = nth(i)
        return 2 * k + y, 2 * k + 1 - y

    def part_copy(b):
        return remote(part_out.at[b], part_in.at[b], part_send.at[b], part_recv.at[b], twin)

    def sum_copy(b):
        return remote(sum_out.at[b], sum_in.at[b], sum_send.at[b], sum_recv.at[b], across)

    def mid_copy(k, slot):
        return remote(
            middle.at[k, slot], middle.at[k, slot], mid_send.at[k, slot], mid_recv.at[k, slot], twin
        )

    def mixer_product(first, b):
        lhs = gated[pl.ds(first, 2)].reshape(2 * rows, width)
        return dot(lhs, g2[b]).reshape(2, rows, model)

    @pl.loop(0, lines + 1)
    def _(i):
        @pl.when(i < lines)
        def _():
            for b in of_unit(i):

                @pl.when(b != f)
                def _():
                    pair_wait(2, b)

                part_out[b] = mixer_product(peers, b).astype(BF16)
                part_copy(b).start()

        @pl.when(i > 0)
        def _():
            for b in of_unit(i - 1):
                value = mixer_product(c * 2, b)
                part_copy(b).wait_recv()
                sum_out[b] = (value + part_in[b].astype(F32)).astype(BF16)
                sum_copy(b).start()

    for s in PHASES[3]:
        cross_pair(s).start()

    @pl.loop(0, lines)
    def _(i):
        @pl.when(i + 1 < lines)
        def _():
            steps(2, i + 1)

        @pl.when(i == lines - 2)
        def _():
            crossed(3)

        @pl.when(i == lines - 1)
        def _():
            steps(3, 1)

        k = nth(i)
        here = pl.ds(pl.multiple_of(k * 2 * model, LANES), 2 * model)
        for side in range(2):
            b = 2 * k + side
            sum_copy(b).wait_recv()
            for j in range(2):
                slot = c * 2 + j
                there = slice(side * model, (side + 1) * model)
                base = rows_in[slot, :, here][:, there].astype(F32)
                total = sum_out[b, j].astype(F32) + sum_in[b, j].astype(F32)
                middle[k, slot, :, there] = (base + total).astype(BF16)
        for j in range(2):
            mid_copy(k, c * 2 + j).start()

    def norm_middle(slot):
        @pl.loop(0, rows // tile)
        def _(i):
            here = pl.ds(pl.multiple_of(i * tile, tile), tile)
            wide = [middle[k, slot, here, :].astype(F32) for k in range(lines)]
            total = sum(jnp.sum(w * w, axis=-1, keepdims=True) for w in wide)
            scale = lax.rsqrt(total / depth + 1e-06)
            for k in range(lines):
                there = slice(k * 2 * model, (k + 1) * 2 * model)
                normed[slot, here, there] = (wide[k] * scale * channel_gain[:, there]).astype(BF16)

    for j in range(2):
        norm_middle(c * 2 + j)
    for j in range(2):

        @pl.loop(0, lines)
        def _(k):
            mid_copy(k, peers + j).wait_recv()

        norm_middle(peers + j)

    for s in PHASES[2]:
        complete(s)

    place = lax.broadcasted_iota(jnp.int32, (rows, units), 0) % SEQ_LEN

    def channel(slot):
        n = normed[slot]
        gates = dot(n, g3[...].reshape(depth, units)).astype(BF16).astype(F32)
        conv = taps_here[KCONV - 1 : KCONV, :] * gates
        for lag in range(1, KCONV):
            shifted = jnp.where(place >= lag, pltpu.roll(gates, lag, 0), 0.0)
            conv = conv + taps_here[KCONV - 1 - lag : KCONV - lag, :] * shifted
        ups = dot(n, g4[...].reshape(depth, units)).astype(BF16).astype(F32)
        hidden[slot] = (jax.nn.silu(conv) * ups).astype(BF16)

    def half_channel(side):
        @pl.loop(0, 2)
        def _(core):
            channel(core * 2 + side)

    @pl.loop(0, fs)
    def _(b):
        part_copy(b).wait_send()
        sum_copy(b).wait_send()

    def last_part(b, side):
        return remote(
            part_out.at[b, side],
            part_in.at[b, side],
            part_send2.at[b, side],
            part_recv2.at[b, side],
            twin,
        )

    def last_copy(b):
        return remote(sum_out.at[b, 0], last_in.at[b], last_send.at[b], last_recv.at[b], across)

    def give(b, side):
        part_out[b, side] = dot(hidden[peers + side], g5[b]).astype(BF16)
        last_part(b, side).start()

    def send_units(first, last):
        @pl.loop(first, last + 1)
        def _(i):
            @pl.when(i < last)
            def _():
                for b in of_unit(i):

                    @pl.when(b != f)
                    def _():
                        pair_wait(5, b)

                    give(b, 1 - y)

            @pl.when(i > first)
            def _():
                for b in of_unit(i - 1):
                    value = dot(hidden[beside], g5[b])
                    last_part(b, 1 - y).wait_recv()
                    sum_out[b, 0] = (value + part_in[b, 1 - y].astype(F32)).astype(BF16)
                    last_copy(b).start()

    half_channel(1 - y)
    split = lines // 2
    reach = min(lines, max(split, 3))
    for d in range(2, reach):
        steps(3, d)
    send_units(0, split)
    half_channel(y)
    for d in range(reach, lines):
        steps(3, d)
    send_units(split, lines)

    @pl.loop(0, lines)
    def _(i):
        for b in of_unit(i):
            give(b, y)

    @pl.loop(0, lines)
    def _(i):
        k = nth(i)
        values = [dot(hidden[mine], g5[2 * k + side]) for side in range(2)]
        for side in range(2):
            b = 2 * k + side
            last_part(b, y).wait_recv()
            last_copy(b).wait_recv()
            total = values[side] + part_in[b, y].astype(F32) + last_in[b].astype(F32)
            there = slice(side * model, (side + 1) * model)
            values[side] = (total + middle[k, mine, :, there].astype(F32)).astype(BF16)
        here = pl.ds(pl.multiple_of(k * 2 * model, LANES), 2 * model)
        out[:, here] = jnp.concatenate(values, axis=1)

    for s in range(STREAMS):
        cross_line(s).wait_send()
        if s in BY_COPY:
            to_copy(s, beyond).wait_send()
        else:
            cross_pair(s).wait_send()

        @pl.when(has_left)
        def _():
            for side in range(2):
                on_line(s, 2 * q + side, left_send.at[s, side], left).wait_send()

        @pl.loop(0, fs)
        def _(source):
            k = source // 2

            @pl.when(((k <= q) & has_right) | ((k > q) & has_left))
            def _():
                on_line(s, source, line_send.at[s, source], across).wait_send()

            @pl.when(k != q)
            def _():
                to_copy(s, source).wait_send()

    for copy in (row_to_across, row_to_twin, row_forward, *stat_copies):
        copy.wait_send()

    @pl.loop(0, fs)
    def _(b):
        for side in range(2):
            last_part(b, side).wait_send()
        last_copy(b).wait_send()

    @pl.loop(0, lines)
    def _(k):
        for j in range(2):
            mid_copy(k, c * 2 + j).wait_send()


def body(reps, fs, tps):
    assert reps == 2 and tps == 2 and fs % 2 == 0

    def on_device(
        residual,
        mixer_gain,
        gating_proj,
        spatial_proj,
        spatial_gain,
        spatial_bias,
        spatial_mix,
        spatial_offset,
        mixer_out,
        channel_gain,
        gate_proj,
        up_proj,
        conv_taps,
        down_proj,
    ):
        rows, depth = residual.shape
        assert rows % SEQ_LEN == 0
        own_rows = gating_proj.shape[0]
        width = gating_proj.shape[1] // 2
        units = gate_proj.shape[1] // 2
        group = gating_proj.shape[1] * tps
        columns = mixer_out.shape[1]
        span = spatial_mix.shape[1]
        heads = width // HEAD
        lines = fs // 2
        vmem, hbm = pl.BlockSpec(memory_space=pltpu.VMEM), pl.BlockSpec(memory_space=pl.ANY)
        dma = pltpu.SemaphoreType.DMA
        return pl.pallas_call(
            functools.partial(kernel, (fs, rows, depth, group, width, units)),
            out_shape=jax.ShapeDtypeStruct((rows, depth), BF16),
            in_specs=[hbm] * 8 + [vmem] * 6,
            out_specs=vmem,
            scratch_shapes=[
                pltpu.VMEM((fs, own_rows, width), BF16),
                pltpu.VMEM((fs, own_rows, width), BF16),
                pltpu.VMEM((fs, width, columns), BF16),
                pltpu.VMEM((fs, own_rows, units), BF16),
                pltpu.VMEM((fs, own_rows, units), BF16),
                pltpu.VMEM((fs, units, columns), BF16),
                pltpu.VMEM((2, own_rows, 2 * units), BF16),
                pltpu.VMEM((2, own_rows, units), BF16),
                pltpu.VMEM((KCONV, units), F32),
                pltpu.VMEM((4, rows, depth), BF16),
                pltpu.VMEM((4, rows, depth), BF16),
                pltpu.VMEM((lines, 4, rows, 2 * columns), BF16),
                pltpu.VMEM((4, rows, width), F32),
                pltpu.VMEM((4, rows, width), F32),
                pltpu.VMEM((4, rows, width), BF16),
                pltpu.VMEM((4, rows, units), BF16),
                pltpu.VMEM((heads, span, span), BF16),
                pltpu.VMEM((heads * HEAD // LANES, span, span * LANES // HEAD), BF16),
                pltpu.VMEM((span, width), F32),
                pltpu.VMEM((4, 2, 4 * rows), F32),
                pltpu.VMEM((fs, 2, rows, columns), BF16),
                pltpu.VMEM((fs, 2, rows, columns), BF16),
                pltpu.VMEM((fs, 2, rows, columns), BF16),
                pltpu.VMEM((fs, 2, rows, columns), BF16),
                pltpu.VMEM((fs, rows, columns), BF16),
                dma((STREAMS + 2,)),
                dma((STREAMS, fs)),
                dma((STREAMS, fs)),
                dma((STREAMS, 2)),
                dma((STREAMS, fs)),
                dma((STREAMS, fs)),
                dma((STREAMS, 2)),
                dma((3,)),
                dma((4,)),
                dma((3,)),
                dma((4,)),
                dma((fs,)),
                dma((fs,)),
                dma((fs,)),
                dma((fs,)),
                dma((lines, 4)),
                dma((lines, 4)),
                dma((fs, 2)),
                dma((fs, 2)),
                dma((fs,)),
                dma((fs,)),
            ],
            compiler_params=pltpu.CompilerParams(
                collective_id=0, has_side_effects=True, vmem_limit_bytes=67043328
            ),
        )(
            residual,
            gating_proj,
            spatial_proj,
            mixer_out,
            gate_proj,
            up_proj,
            down_proj,
            spatial_mix,
            mixer_gain.reshape(1, -1),
            channel_gain.reshape(1, -1),
            spatial_gain.reshape(1, -1),
            spatial_bias.reshape(1, -1),
            spatial_offset,
            conv_taps,
        )

    return on_device


def solution(mesh):
    in_specs = (
        P(("rep", "fs", "tp"), None),
        P(),
        P("fs", "tp"),
        P("fs", "tp"),
        P(),
        P(),
        P(),
        P(),
        P("tp", "fs"),
        P(),
        P("fs", "tp"),
        P("fs", "tp"),
        P(),
        P("tp", "fs"),
    )
    out_specs = P(("rep", "fs", "tp"), None)
    return jax.shard_map(
        body(mesh.shape["rep"], mesh.shape["fs"], mesh.shape["tp"]),
        mesh=mesh,
        in_specs=in_specs,
        out_specs=out_specs,
        check_vma=False,
    )
```

time: 226 us -> 177 us (0.78)
  Pallas kernels: 220 us -> 175 us
  local copies, waits for them, and re-layouts: 6.18 us -> 2.3 us
    pallas_call x1, Pallas kernels: 220 us -> 175 us  [on_device(): pl.pallas_call(functools.partial(kernel, (fs, rows, depth, group, width,...]
    dynamic_slice x2 -> x0, local copies, waits for them, and re-layouts: 3.88 us -> none  [the longest x1 2.49 us: on_device(): up_here = lax.dynamic_slice_in_dim(up_proj, r * units, units, 1)]
where the time goes in v1:
time: 177 us
  Pallas kernels  175 us (99%)
  local copies, waits for them, and re-layouts  2.3 us (1%)
    pallas_call x1, Pallas kernels, on_device(): pl.pallas_call(functools.partial(kernel, (fs, rows, depth, group, width,...  175 us

profile of v1, /device:TPU:0, one launch (start us, length us, event | category | flops | bytes accessed | tf_op | source)
XLA Modules:
  0.0 177.1 jit_solution(789032997046718702)
XLA Ops:
  0.0 174.8 %shard_map.136 = bf16[256,2048]{1,0:T(8,128)(2,1)} custom-call(bf16[256,2048]{1,0:T(8,128)(2,1)} %residual.1, bf16[256,1024]{1,0:T(8,128)(2,1)} %gating.1, bf16[256,1024]{1,0:T(8,128)(2,1)} %spatial.1, bf16[1024,256]{1,0:T(8,128)(2,1)} %mixer_out.1, bf16[256,1408]{1,0:T(8,128)(2,1)} %gate.1, bf16[256,1408]{1,0:T(8,128)(2,1)} %up.1, bf16[1408,256]{1,0:T(8,128)(2,1)} %down.1, ...), custom_call_target="tpu_custom_call" | custom-call | tf_op jit(solution)/shard_map/pallas_call | solution.py:690
  174.8 2.3 %copy.16 = bf16[256,2048]{1,0:T(8,128)(2,1)} copy(bf16[256,2048]{1,0:T(8,128)(2,1)} %shard_map.136) | data formatting | bytes 2097152

commit v2 on v1

--- a/solution.py
+++ b/solution.py
@@ -18,7 +18,7 @@
 
 PHASES = ((0, 1), (2,), (3, 4), (5,))
 STREAMS = 6
-BY_COPY = (3, 4)
+BY_COPY = (0, 1)
 
 
 def dot(a, b):
@@ -45,8 +45,7 @@
     g0,
     g1,
     g2,
-    g3,
-    g4,
+    g34,
     g5,
     raw,
     cross,
@@ -67,7 +66,9 @@
     sum_out,
     sum_in,
     last_in,
+    out_here,
     local_sem,
+    out_sem,
     line_recv,
     pair_recv,
     left_send,
@@ -91,8 +92,10 @@
 ):
     fs, rows, depth, group, width, units = dims
     lines = fs // 2
-    blocks = (g0, g1, g2, g3, g4, g5)
+    blocks = (g0, g1, g2, g34, g34, g5)
     halves = [block.shape[1] // 2 for block in blocks]
+    sizes = [size // 2 if s in PHASES[2] else size for s, size in enumerate(halves)]
+    starts = [sizes[s] if s == PHASES[2][1] else 0 for s in range(STREAMS)]
     r, f, c = lax.axis_index("rep"), lax.axis_index("fs"), lax.axis_index("tp")
     q, y = f // 2, f % 2
     beyond = f + 1 - 2 * y
@@ -150,7 +153,7 @@
     pl.semaphore_wait(barrier, 4 + jnp.minimum(q, 1) + jnp.minimum(lines - 1 - q, 1))
 
     def half(s, source, h):
-        return blocks[s].at[source, at(h * halves[s], halves[s], 16)]
+        return blocks[s].at[source, at(h * halves[s] + starts[s], sizes[s], 16)]
 
     def on_line(s, source, send, device):
         ref = half(s, source, r)
@@ -177,7 +180,7 @@
         elif s == 2:
             src = mixer_out.at[at(start + h * halves[s], halves[s], 16)]
         elif s < 5:
-            src = cross.at[s - 3, here]
+            src = cross.at[at(h * halves[s] + starts[s], sizes[s], 16)]
         else:
             src = down.at[at((1 - y) * units + h * halves[s], halves[s], 16)]
         return src, half(s, f, h)
@@ -210,8 +213,11 @@
             if s in BY_COPY:
                 to_copy(s, beyond).start()
 
-    def step(s, d, other):
-        @pl.when(q - d >= 0)
+    near = jnp.minimum(q, lines - 1 - q)
+    at_end, inside = near == 0, near > 0
+
+    def step(s, d, other, who):
+        @pl.when((q - d >= 0) & who)
         def _():
             source = (beyond if other else f) - 2 * d
             line_wait(s, source)
@@ -222,7 +228,7 @@
 
             to_copy(s, source).start()
 
-        @pl.when(q + d < lines)
+        @pl.when((q + d < lines) & who)
         def _():
             source = (beyond if other else f) + 2 * d
             line_wait(s, source)
@@ -233,10 +239,14 @@
 
             to_copy(s, source).start()
 
-    def steps(p, d):
-        for other in (False, True):
+    def steps(p, d, who=True, others=(False, True)):
+        for other in others:
             for s in PHASES[p]:
-                step(s, d, other)
+                step(s, d, other, who)
+
+    def steps_from(p, first, who):
+        for d in range(first, lines):
+            steps(p, d, who)
 
     def complete(s):
         @pl.loop(0, fs)
@@ -252,11 +262,8 @@
     row_to_across.start()
     row_to_twin.start()
     for s in PHASES[0]:
-        cross_pair(s).start()
-    for p in range(2):
-        for s in PHASES[p]:
-            own_copies[s].wait()
-        own(p)
+        own_copies[s].wait()
+    own(0)
 
     def row_wait(slot):
         remote(
@@ -273,14 +280,20 @@
             scale = lax.rsqrt(jnp.mean(wide * wide, axis=-1, keepdims=True) + 1e-06)
             normed[slot, here, :] = (wide * scale * mixer_gain[...]).astype(BF16)
 
-    for i, s in enumerate(PHASES[2]):
+    main = units // LANES * LANES
+    rest = units - main
+    for s in PHASES[2]:
         own_copies[s].wait()
-        for way in range(2):
-
-            @pl.when(y == way)
-            def _():
-                blocks[s][f] = raw[i, :, way * units : (way + 1) * units]
-                cross[i] = raw[i, :, (1 - way) * units : (2 - way) * units]
+    for way in range(2):
+
+        @pl.when(y == way)
+        def _():
+            for i in range(2):
+                for ref, first in ((g34.at[f], way * units), (cross, (1 - way) * units)):
+                    ref[:, i * main : (i + 1) * main] = raw[i, :, first : first + main]
+                    if rest:
+                        there = slice(2 * main + i * rest, 2 * main + (i + 1) * rest)
+                        ref[:, there] = raw[i, :, first + main : first + units]
 
     for k in range(4):
 
@@ -288,27 +301,30 @@
         def _():
             taps_here[...] = taps[:, k * units : (k + 1) * units]
 
-    for s in PHASES[2] + PHASES[1] + PHASES[3]:
-        if s in PHASES[1]:
-            cross_pair(s).start()
-        else:
-            cross_line(s).start()
     row_copy.wait()
     norm_in(mine)
+    own_copies[2].wait()
     own_copies[5].wait()
     mix_copy.wait()
 
     crossed(0)
     for d in range(1, lines - 1):
         steps(0, d)
+    own(1)
+    crossed(1)
+    for s in PHASES[2]:
+        cross_line(s).start()
+    steps(0, lines - 1)
     row_wait(beside)
     row_forward = remote(
         rows_in.at[beside], rows_in.at[beside], row_send.at[2], row_recv.at[beside], twin
     )
     row_forward.start()
     norm_in(beside)
-    steps(0, lines - 1)
-    crossed(1)
+    for s in PHASES[1] + PHASES[2]:
+        cross_pair(s).start()
+    steps(1, 1)
+    steps_from(1, 2, inside)
     own(2)
     for j in range(2):
         row_wait(peers + j)
@@ -359,16 +375,22 @@
             stat[mine, 0:1, here] = row_of(total[b * span : (b + 1) * span])
             stat[mine, 1:2, here] = row_of(squares[b * span : (b + 1) * span])
 
+    last = lines - 1
+
     @pl.loop(0, 4)
     def _(slot):
         project(slot)
 
-        @pl.when(slot + 1 < lines)
-        def _():
-            steps(1, slot + 1)
-
-    for d in range(5, lines):
-        steps(1, d)
+        @pl.when(slot == 1)
+        def _():
+            crossed(2)
+            for d in range(2, last):
+                steps(1, d, at_end, (False,))
+
+        @pl.when(slot == 2)
+        def _():
+            for d in range(2, last):
+                steps(1, d, at_end, (True,))
 
     stat_copies = [
         remote(stat.at[mine], stat.at[mine], stat_send.at[i], stat_recv.at[mine], device)
@@ -376,8 +398,9 @@
     ]
     for copy in stat_copies:
         copy.start()
-    crossed(2)
-    own(3)
+    for s in PHASES[3]:
+        cross_line(s).start()
+    steps(1, last, at_end & (last > 1))
     for other in (beside, peers, peers + 1):
         remote(
             stat.at[other], stat.at[other], stat_send.at[0], stat_recv.at[other], across
@@ -425,8 +448,6 @@
         gate_slot(slot)
 
     model = g2.shape[2]
-    near = jnp.minimum(q, lines - 1 - q)
-
     def nth(i):
         d = (i + 1) // 2
         close = jnp.where(i % 2 == 1, q + d, q - d)
@@ -473,22 +494,48 @@
                 sum_out[b] = (value + part_in[b].astype(F32)).astype(BF16)
                 sum_copy(b).start()
 
+        @pl.when(i == 1)
+        def _():
+            steps(2, 1, inside, (False,))
+
+        @pl.when(i == 2)
+        def _():
+            steps(2, 1, inside, (True,))
+
+        @pl.when(i == lines - 1)
+        def _():
+            steps(2, 1, at_end, (False,))
+
     for s in PHASES[3]:
         cross_pair(s).start()
 
     @pl.loop(0, lines)
     def _(i):
-        @pl.when(i + 1 < lines)
-        def _():
-            steps(2, i + 1)
+        @pl.when(i == 0)
+        def _():
+            for d in range(2, lines):
+                steps(2, d, inside, (False,))
+            steps(2, 1, at_end, (True,))
+
+        @pl.when(i == 1)
+        def _():
+            for d in range(2, lines):
+                steps(2, d, inside, (True,))
+            for d in range(2, last):
+                steps(2, d, at_end, (False,))
+            own(3)
+            crossed(3)
 
         @pl.when(i == lines - 2)
         def _():
-            crossed(3)
+            for d in range(2, last):
+                steps(2, d, at_end, (True,))
+            steps(2, last, at_end & (last > 1), (False,))
 
         @pl.when(i == lines - 1)
         def _():
-            steps(3, 1)
+            steps(3, 1, inside)
+            steps(2, last, at_end & (last > 1), (True,))
 
         k = nth(i)
         here = pl.ds(pl.multiple_of(k * 2 * model, LANES), 2 * model)
@@ -515,6 +562,7 @@
                 there = slice(k * 2 * model, (k + 1) * 2 * model)
                 normed[slot, here, there] = (wide[k] * scale * channel_gain[:, there]).astype(BF16)
 
+    steps_from(3, 2, inside)
     for j in range(2):
         norm_middle(c * 2 + j)
     for j in range(2):
@@ -525,20 +573,25 @@
 
         norm_middle(peers + j)
 
+    steps(3, 1, at_end)
     for s in PHASES[2]:
         complete(s)
 
-    place = lax.broadcasted_iota(jnp.int32, (rows, units), 0) % SEQ_LEN
-
     def channel(slot):
-        n = normed[slot]
-        gates = dot(n, g3[...].reshape(depth, units)).astype(BF16).astype(F32)
-        conv = taps_here[KCONV - 1 : KCONV, :] * gates
-        for lag in range(1, KCONV):
-            shifted = jnp.where(place >= lag, pltpu.roll(gates, lag, 0), 0.0)
-            conv = conv + taps_here[KCONV - 1 - lag : KCONV - lag, :] * shifted
-        ups = dot(n, g4[...].reshape(depth, units)).astype(BF16).astype(F32)
-        hidden[slot] = (jax.nn.silu(conv) * ups).astype(BF16)
+        both = dot(normed[slot], g34[...].reshape(depth, 2 * units))
+        pieces = [(0, main, 0, main)]
+        if rest:
+            pieces.append((main, units, 2 * main, 2 * main + rest))
+        for first, end, gate_at, up_at in pieces:
+            size = end - first
+            gates = both[:, gate_at : gate_at + size].astype(BF16).astype(F32)
+            ups = both[:, up_at : up_at + size].astype(BF16).astype(F32)
+            place = lax.broadcasted_iota(jnp.int32, (rows, size), 0) % SEQ_LEN
+            conv = taps_here[KCONV - 1 : KCONV, first:end] * gates
+            for lag in range(1, KCONV):
+                shifted = jnp.where(place >= lag, pltpu.roll(gates, lag, 0), 0.0)
+                conv = conv + taps_here[KCONV - 1 - lag : KCONV - lag, first:end] * shifted
+            hidden[slot, :, first:end] = (jax.nn.silu(conv) * ups).astype(BF16)
 
     def half_channel(side):
         @pl.loop(0, 2)
@@ -562,46 +615,62 @@
     def last_copy(b):
         return remote(sum_out.at[b, 0], last_in.at[b], last_send.at[b], last_recv.at[b], across)
 
+    def of_block(i):
+        return 2 * nth(i // 2) + jnp.where(i % 2 == 0, y, 1 - y)
+
     def give(b, side):
         part_out[b, side] = dot(hidden[peers + side], g5[b]).astype(BF16)
         last_part(b, side).start()
 
-    def send_units(first, last):
-        @pl.loop(first, last + 1)
+    def give_both(b):
+        lhs = hidden[pl.ds(peers, 2)].reshape(2 * rows, units)
+        part_out[b] = dot(lhs, g5[b]).reshape(2, rows, model).astype(BF16)
+        for side in range(2):
+            last_part(b, side).start()
+
+    def send_blocks(first, end, both):
+        @pl.loop(first, end + 1)
         def _(i):
-            @pl.when(i < last)
+            @pl.when(i < end)
             def _():
-                for b in of_unit(i):
-
-                    @pl.when(b != f)
-                    def _():
-                        pair_wait(5, b)
-
+                b = of_block(i)
+
+                @pl.when(b != f)
+                def _():
+                    pair_wait(5, b)
+
+                if both:
+                    give_both(b)
+                else:
                     give(b, 1 - y)
 
             @pl.when(i > first)
             def _():
-                for b in of_unit(i - 1):
-                    value = dot(hidden[beside], g5[b])
-                    last_part(b, 1 - y).wait_recv()
-                    sum_out[b, 0] = (value + part_in[b, 1 - y].astype(F32)).astype(BF16)
-                    last_copy(b).start()
+                b = of_block(i - 1)
+                value = dot(hidden[beside], g5[b])
+                last_part(b, 1 - y).wait_recv()
+                sum_out[b, 0] = (value + part_in[b, 1 - y].astype(F32)).astype(BF16)
+                last_copy(b).start()
 
     half_channel(1 - y)
     split = lines // 2
     reach = min(lines, max(split, 3))
     for d in range(2, reach):
-        steps(3, d)
-    send_units(0, split)
+        steps(3, d, at_end)
+    send_blocks(0, 2 * split, False)
     half_channel(y)
+
+    @pl.loop(0, 2 * split)
+    def _(i):
+        give(of_block(i), y)
+
     for d in range(reach, lines):
-        steps(3, d)
-    send_units(split, lines)
-
-    @pl.loop(0, lines)
-    def _(i):
-        for b in of_unit(i):
-            give(b, y)
+        steps(3, d, at_end)
+    send_blocks(2 * split, fs, True)
+
+    def out_copy(k):
+        here = pl.ds(pl.multiple_of(k * 2 * model, LANES), 2 * model)
+        return pltpu.make_async_copy(out_here.at[k], out.at[:, here], out_sem.at[k])
 
     @pl.loop(0, lines)
     def _(i):
@@ -613,9 +682,9 @@
             last_copy(b).wait_recv()
             total = values[side] + part_in[b, y].astype(F32) + last_in[b].astype(F32)
             there = slice(side * model, (side + 1) * model)
-            values[side] = (total + middle[k, mine, :, there].astype(F32)).astype(BF16)
-        here = pl.ds(pl.multiple_of(k * 2 * model, LANES), 2 * model)
-        out[:, here] = jnp.concatenate(values, axis=1)
+            total = total + middle[k, mine, :, there].astype(F32)
+            out_here[k, :, there] = total.astype(BF16)
+        out_copy(k).start()
 
     for s in range(STREAMS):
         cross_line(s).wait_send()
@@ -654,6 +723,7 @@
     def _(k):
         for j in range(2):
             mid_copy(k, c * 2 + j).wait_send()
+        out_copy(k).wait()
 
 
 def body(reps, fs, tps):
@@ -691,16 +761,15 @@
             functools.partial(kernel, (fs, rows, depth, group, width, units)),
             out_shape=jax.ShapeDtypeStruct((rows, depth), BF16),
             in_specs=[hbm] * 8 + [vmem] * 6,
-            out_specs=vmem,
+            out_specs=hbm,
             scratch_shapes=[
                 pltpu.VMEM((fs, own_rows, width), BF16),
                 pltpu.VMEM((fs, own_rows, width), BF16),
                 pltpu.VMEM((fs, width, columns), BF16),
-                pltpu.VMEM((fs, own_rows, units), BF16),
-                pltpu.VMEM((fs, own_rows, units), BF16),
+                pltpu.VMEM((fs, own_rows, 2 * units), BF16),
                 pltpu.VMEM((fs, units, columns), BF16),
                 pltpu.VMEM((2, own_rows, 2 * units), BF16),
-                pltpu.VMEM((2, own_rows, units), BF16),
+                pltpu.VMEM((own_rows, 2 * units), BF16),
                 pltpu.VMEM((KCONV, units), F32),
                 pltpu.VMEM((4, rows, depth), BF16),
                 pltpu.VMEM((4, rows, depth), BF16),
@@ -718,7 +787,9 @@
                 pltpu.VMEM((fs, 2, rows, columns), BF16),
                 pltpu.VMEM((fs, 2, rows, columns), BF16),
                 pltpu.VMEM((fs, rows, columns), BF16),
+                pltpu.VMEM((lines, rows, 2 * columns), BF16),
                 dma((STREAMS + 2,)),
+                dma((lines,)),
                 dma((STREAMS, fs)),
                 dma((STREAMS, fs)),
                 dma((STREAMS, 2)),

time: 177 us -> 158 us (0.89)
  Pallas kernels: 175 us -> 156 us
    pallas_call x1, Pallas kernels: 175 us -> 156 us  [on_device(): pl.pallas_call(functools.partial(kernel, (fs, rows, depth, group, width,...]
where the time goes in v2:
time: 158 us
  Pallas kernels  156 us (99%)
  local copies, waits for them, and re-layouts  2.3 us (1%)
    pallas_call x1, Pallas kernels, on_device(): pl.pallas_call(functools.partial(kernel, (fs, rows, depth, group, width,...  156 us

profile of v2, /device:TPU:0, one launch (start us, length us, event | category | flops | bytes accessed | tf_op | source)
XLA Modules:
  0.0 158.2 jit_solution(6624627760941524549)
XLA Ops:
  0.0 155.9 %shard_map.136 = bf16[256,2048]{1,0:T(8,128)(2,1)} custom-call(bf16[256,2048]{1,0:T(8,128)(2,1)} %residual.1, bf16[256,1024]{1,0:T(8,128)(2,1)} %gating.1, bf16[256,1024]{1,0:T(8,128)(2,1)} %spatial.1, bf16[1024,256]{1,0:T(8,128)(2,1)} %mixer_out.1, bf16[256,1408]{1,0:T(8,128)(2,1)} %gate.1, bf16[256,1408]{1,0:T(8,128)(2,1)} %up.1, bf16[1408,256]{1,0:T(8,128)(2,1)} %down.1, ...), custom_call_target="tpu_custom_call" | custom-call | tf_op jit(solution)/shard_map/pallas_call | solution.py:760
  155.9 2.3 %copy.16 = bf16[256,2048]{1,0:T(8,128)(2,1)} copy(bf16[256,2048]{1,0:T(8,128)(2,1)} %shard_map.136) | data formatting | bytes 2097152

commit v3 on v2

--- a/solution.py
+++ b/solution.py
@@ -18,7 +18,6 @@
 
 PHASES = ((0, 1), (2,), (3, 4), (5,))
 STREAMS = 6
-BY_COPY = (0, 1)
 
 
 def dot(a, b):
@@ -70,9 +69,10 @@
     local_sem,
     out_sem,
     line_recv,
-    pair_recv,
+    pair_each,
+    pair_all,
     left_send,
-    line_send,
+    right_send,
     pair_send,
     cross_send,
     row_send,
@@ -159,18 +159,26 @@
         ref = half(s, source, r)
         return remote(ref, ref, send, line_recv.at[s, source], device)
 
+    def pair_sem(s, source):
+        each = PHASES[1] + PHASES[3]
+        return pair_each.at[each.index(s), source] if s in each else pair_all.at[s]
+
     def to_copy(s, source):
         ref = half(s, source, r)
-        return remote(ref, ref, pair_send.at[s, source], pair_recv.at[s, source], copy_chip)
+        return remote(ref, ref, pair_send.at[s], pair_sem(s, source), copy_chip)
 
     def line_wait(s, source):
-        on_line(s, source, line_send.at[s, source], across).wait_recv()
+        on_line(s, source, left_send.at[s], across).wait_recv()
 
     def pair_wait(s, source):
         ref = half(s, source, 1 - r)
-        remote(
-            ref, ref, pair_send.at[s, source], pair_recv.at[s, source], copy_chip
-        ).wait_recv()
+        remote(ref, ref, pair_send.at[s], pair_sem(s, source), copy_chip).wait_recv()
+
+    def bulk(ref, sem):
+        return remote(ref, ref, sem, sem, across)
+
+    def chunks(s, count, sem):
+        return bulk(blocks[s].at[pl.ds(0, count), pl.ds(0, sizes[s])], sem)
 
     def crossing(s, h):
         start = (1 - y) * width
@@ -187,31 +195,29 @@
 
     def cross_line(s):
         src, dst = crossing(s, r)
-        return remote(src, dst, cross_send.at[s, 0], line_recv.at[s, f], across)
+        return remote(src, dst, cross_send.at[s], line_recv.at[s, f], across)
 
     def cross_pair(s):
         src, dst = crossing(s, 1 - r)
-        return remote(src, dst, cross_send.at[s, 1], pair_recv.at[s, f], across)
+        return remote(src, dst, cross_send.at[s], pair_sem(s, f), across)
 
     def both_ways(s, source):
         @pl.when(has_left)
         def _():
-            on_line(s, source, left_send.at[s, source % 2], left).start()
+            on_line(s, source, left_send.at[s], left).start()
 
         @pl.when(has_right)
         def _():
-            on_line(s, source, line_send.at[s, source], right).start()
+            on_line(s, source, right_send.at[s], right).start()
 
     def own(p):
         for s in PHASES[p]:
             both_ways(s, f)
 
-    def crossed(p):
-        for s in PHASES[p]:
+    def crossed(p, only=None):
+        for s in PHASES[p] if only is None else (only,):
             line_wait(s, beyond)
             both_ways(s, beyond)
-            if s in BY_COPY:
-                to_copy(s, beyond).start()
 
     near = jnp.minimum(q, lines - 1 - q)
     at_end, inside = near == 0, near > 0
@@ -224,7 +230,7 @@
 
             @pl.when(has_right)
             def _():
-                on_line(s, source, line_send.at[s, source], right).start()
+                on_line(s, source, right_send.at[s], right).start()
 
             to_copy(s, source).start()
 
@@ -235,7 +241,7 @@
 
             @pl.when(has_left)
             def _():
-                on_line(s, source, line_send.at[s, source], left).start()
+                on_line(s, source, left_send.at[s], left).start()
 
             to_copy(s, source).start()
 
@@ -249,25 +255,22 @@
             steps(p, d, who)
 
     def complete(s):
-        @pl.loop(0, fs)
-        def _(source):
-            @pl.when(source != f)
-            def _():
-                pair_wait(s, source)
-
-    row_to_across = remote(residual, rows_in.at[mine], row_send.at[0], row_recv.at[mine], across)
-    row_to_twin = remote(residual, rows_in.at[mine], row_send.at[1], row_recv.at[mine], twin)
+        chunks(s, fs - 1, pair_all.at[s]).wait_recv()
+
+    row_to_across = remote(residual, rows_in.at[mine], row_send, row_recv.at[mine], across)
+    row_to_twin = remote(residual, rows_in.at[mine], row_send, row_recv.at[mine], twin)
     for s in PHASES[0] + PHASES[1]:
         cross_line(s).start()
     row_to_across.start()
     row_to_twin.start()
     for s in PHASES[0]:
+        cross_pair(s).start()
         own_copies[s].wait()
     own(0)
 
     def row_wait(slot):
         remote(
-            rows_in.at[slot], rows_in.at[slot], row_send.at[0], row_recv.at[slot], across
+            rows_in.at[slot], rows_in.at[slot], row_send, row_recv.at[slot], across
         ).wait_recv()
 
     tile = 64
@@ -307,28 +310,33 @@
     own_copies[5].wait()
     mix_copy.wait()
 
-    crossed(0)
+    for s in PHASES[0]:
+        step(s, 1, False, True)
+        crossed(0, s)
     for d in range(1, lines - 1):
-        steps(0, d)
+        for s in PHASES[0]:
+            step(s, d + 1, False, True)
+            step(s, d, True, True)
     own(1)
     crossed(1)
     for s in PHASES[2]:
         cross_line(s).start()
-    steps(0, lines - 1)
+    steps(0, lines - 1, True, (True,))
     row_wait(beside)
     row_forward = remote(
-        rows_in.at[beside], rows_in.at[beside], row_send.at[2], row_recv.at[beside], twin
+        rows_in.at[beside], rows_in.at[beside], row_send, row_recv.at[beside], twin
     )
     row_forward.start()
     norm_in(beside)
-    for s in PHASES[1] + PHASES[2]:
+    for s in PHASES[1]:
         cross_pair(s).start()
-    steps(1, 1)
-    steps_from(1, 2, inside)
-    own(2)
+    steps(1, 1, inside)
     for j in range(2):
         row_wait(peers + j)
         norm_in(peers + j)
+    steps_from(1, 2, inside)
+    own(2)
+    steps(1, 1, at_end)
 
     span = mixw.shape[1]
     per = LANES // HEAD
@@ -362,11 +370,9 @@
     for s in PHASES[0]:
         complete(s)
 
-    def project(slot):
-        n = normed[slot]
-        u = dot(n, g0[...].reshape(depth, width)).astype(BF16).astype(F32)
-        act_u[slot] = jax.nn.gelu(u)
-        v = jax.nn.gelu(dot(n, g1[...].reshape(depth, width)).astype(BF16).astype(F32))
+    def project_v(slot):
+        v = dot(normed[slot], g1[...].reshape(depth, width)).astype(BF16).astype(F32)
+        v = jax.nn.gelu(v)
         act_v[slot] = v
         total = jnp.sum(v, axis=-1, keepdims=True)
         squares = jnp.sum(v * v, axis=-1, keepdims=True)
@@ -375,35 +381,40 @@
             stat[mine, 0:1, here] = row_of(total[b * span : (b + 1) * span])
             stat[mine, 1:2, here] = row_of(squares[b * span : (b + 1) * span])
 
+    def project_u(slot):
+        u = dot(normed[slot], g0[...].reshape(depth, width)).astype(BF16).astype(F32)
+        act_u[slot] = jax.nn.gelu(u)
+
     last = lines - 1
 
     @pl.loop(0, 4)
     def _(slot):
-        project(slot)
-
-        @pl.when(slot == 1)
+        project_v(slot)
+
+        @pl.when(slot == 3)
         def _():
             crossed(2)
             for d in range(2, last):
                 steps(1, d, at_end, (False,))
 
-        @pl.when(slot == 2)
+    for device in (across, twin, diag):
+        remote(stat.at[mine], stat.at[mine], stat_send, stat_recv.at[mine], device).start()
+    cross_pair(PHASES[2][0]).start()
+
+    @pl.loop(0, 4)
+    def _(slot):
+        project_u(slot)
+
+        @pl.when(slot == 1)
         def _():
             for d in range(2, last):
                 steps(1, d, at_end, (True,))
 
-    stat_copies = [
-        remote(stat.at[mine], stat.at[mine], stat_send.at[i], stat_recv.at[mine], device)
-        for i, device in enumerate((across, twin, diag))
-    ]
-    for copy in stat_copies:
-        copy.start()
     for s in PHASES[3]:
         cross_line(s).start()
-    steps(1, last, at_end & (last > 1))
     for other in (beside, peers, peers + 1):
         remote(
-            stat.at[other], stat.at[other], stat_send.at[0], stat_recv.at[other], across
+            stat.at[other], stat.at[other], stat_send, stat_recv.at[other], across
         ).wait_recv()
 
     gain_here = spatial_gain[:, pl.ds(pl.multiple_of(mine * width, LANES), width)]
@@ -454,59 +465,66 @@
         far = jnp.where(q < lines - 1 - q, i, lines - 1 - i)
         return jnp.where(i <= 2 * near, close, far)
 
-    def of_unit(i):
-        k = nth(i)
-        return 2 * k + y, 2 * k + 1 - y
+    def of_block(i):
+        return 2 * nth(i // 2) + jnp.where(i % 2 == 0, y, 1 - y)
 
     def part_copy(b):
-        return remote(part_out.at[b], part_in.at[b], part_send.at[b], part_recv.at[b], twin)
+        return remote(part_out.at[b], part_in.at[b], part_send, part_recv.at[b], twin)
 
     def sum_copy(b):
-        return remote(sum_out.at[b], sum_in.at[b], sum_send.at[b], sum_recv.at[b], across)
+        return remote(sum_out.at[b], sum_in.at[b], sum_send, sum_recv.at[b], across)
 
     def mid_copy(k, slot):
         return remote(
-            middle.at[k, slot], middle.at[k, slot], mid_send.at[k, slot], mid_recv.at[k, slot], twin
+            middle.at[k, slot], middle.at[k, slot], mid_send, mid_recv.at[slot], twin
         )
 
     def mixer_product(first, b):
         lhs = gated[pl.ds(first, 2)].reshape(2 * rows, width)
         return dot(lhs, g2[b]).reshape(2, rows, model)
 
-    @pl.loop(0, lines + 1)
+    @pl.loop(0, fs + 1)
     def _(i):
-        @pl.when(i < lines)
-        def _():
-            for b in of_unit(i):
-
-                @pl.when(b != f)
-                def _():
-                    pair_wait(2, b)
-
-                part_out[b] = mixer_product(peers, b).astype(BF16)
-                part_copy(b).start()
+        @pl.when(i < fs)
+        def _():
+            b = of_block(i)
+
+            @pl.when(b != f)
+            def _():
+                pair_wait(2, b)
+
+            part_out[b] = mixer_product(peers, b).astype(BF16)
+            part_copy(b).start()
 
         @pl.when(i > 0)
         def _():
-            for b in of_unit(i - 1):
-                value = mixer_product(c * 2, b)
-                part_copy(b).wait_recv()
-                sum_out[b] = (value + part_in[b].astype(F32)).astype(BF16)
-                sum_copy(b).start()
+            b = of_block(i - 1)
+            value = mixer_product(c * 2, b)
+            part_copy(b).wait_recv()
+            sum_out[b] = (value + part_in[b].astype(F32)).astype(BF16)
+            sum_copy(b).start()
 
         @pl.when(i == 1)
         def _():
+            steps(1, last, at_end & (last > 1))
+
+        @pl.when(i == 3)
+        def _():
             steps(2, 1, inside, (False,))
 
-        @pl.when(i == 2)
+        @pl.when(i == 5)
         def _():
             steps(2, 1, inside, (True,))
 
-        @pl.when(i == lines - 1)
-        def _():
-            steps(2, 1, at_end, (False,))
-
-    for s in PHASES[3]:
+        @pl.when(i == fs // 2)
+        def _():
+            step(PHASES[2][0], 1, False, at_end)
+
+        @pl.when(i == fs - 1)
+        def _():
+            step(PHASES[2][1], 1, False, at_end)
+
+    for s in PHASES[2][1:] + PHASES[3]:
         cross_pair(s).start()
 
     @pl.loop(0, lines)
@@ -566,11 +584,7 @@
     for j in range(2):
         norm_middle(c * 2 + j)
     for j in range(2):
-
-        @pl.loop(0, lines)
-        def _(k):
-            mid_copy(k, peers + j).wait_recv()
-
+        bulk(middle.at[:, peers + j], mid_recv.at[peers + j]).wait_recv()
         norm_middle(peers + j)
 
     steps(3, 1, at_end)
@@ -593,30 +607,20 @@
                 conv = conv + taps_here[KCONV - 1 - lag : KCONV - lag, first:end] * shifted
             hidden[slot, :, first:end] = (jax.nn.silu(conv) * ups).astype(BF16)
 
-    def half_channel(side):
-        @pl.loop(0, 2)
-        def _(core):
-            channel(core * 2 + side)
-
-    @pl.loop(0, fs)
-    def _(b):
-        part_copy(b).wait_send()
-        sum_copy(b).wait_send()
+    bulk(part_out, part_send).wait_send()
+    bulk(sum_out, sum_send).wait_send()
 
     def last_part(b, side):
         return remote(
             part_out.at[b, side],
             part_in.at[b, side],
-            part_send2.at[b, side],
+            part_send2,
             part_recv2.at[b, side],
             twin,
         )
 
     def last_copy(b):
-        return remote(sum_out.at[b, 0], last_in.at[b], last_send.at[b], last_recv.at[b], across)
-
-    def of_block(i):
-        return 2 * nth(i // 2) + jnp.where(i % 2 == 0, y, 1 - y)
+        return remote(sum_out.at[b, 0], last_in.at[b], last_send, last_recv.at[b], across)
 
     def give(b, side):
         part_out[b, side] = dot(hidden[peers + side], g5[b]).astype(BF16)
@@ -628,45 +632,64 @@
         for side in range(2):
             last_part(b, side).start()
 
-    def send_blocks(first, end, both):
-        @pl.loop(first, end + 1)
+    def pass_on(b):
+        value = dot(hidden[beside], g5[b])
+        last_part(b, 1 - y).wait_recv()
+        sum_out[b, 0] = (value + part_in[b, 1 - y].astype(F32)).astype(BF16)
+        last_copy(b).start()
+
+    def send_blocks(first, end):
+        @pl.loop(first, end)
         def _(i):
-            @pl.when(i < end)
-            def _():
-                b = of_block(i)
-
-                @pl.when(b != f)
-                def _():
-                    pair_wait(5, b)
-
-                if both:
-                    give_both(b)
-                else:
-                    give(b, 1 - y)
-
-            @pl.when(i > first)
-            def _():
-                b = of_block(i - 1)
-                value = dot(hidden[beside], g5[b])
-                last_part(b, 1 - y).wait_recv()
-                sum_out[b, 0] = (value + part_in[b, 1 - y].astype(F32)).astype(BF16)
-                last_copy(b).start()
-
-    half_channel(1 - y)
+            b = of_block(i)
+            pair_wait(5, b)
+            give_both(b)
+            pass_on(b)
+
+    most = (last,) if last > 1 else ()
+    channel(1 - y)
+
+    @pl.when(c == 1)
+    def _():
+        give(f, 1 - y)
+
+    @pl.when(c == 0)
+    def _():
+        pass_on(f)
+
+    for d in range(2, last):
+        steps(3, d, at_end, (False,))
+    channel(3 - y)
+
+    @pl.when(c == 0)
+    def _():
+        give(f, 1 - y)
+
+    pair_wait(5, beyond)
+    give(beyond, 1 - y)
+
+    @pl.when(c == 1)
+    def _():
+        pass_on(f)
+
+    pass_on(beyond)
+    for d in range(2, last):
+        steps(3, d, at_end, (True,))
+
+    @pl.loop(0, 2)
+    def _(core):
+        channel(core * 2 + y)
+
+    for d in most:
+        steps(3, d, at_end, (False,))
+    give(f, y)
+    give(beyond, y)
     split = lines // 2
-    reach = min(lines, max(split, 3))
-    for d in range(2, reach):
-        steps(3, d, at_end)
-    send_blocks(0, 2 * split, False)
-    half_channel(y)
-
-    @pl.loop(0, 2 * split)
-    def _(i):
-        give(of_block(i), y)
-
-    for d in range(reach, lines):
-        steps(3, d, at_end)
-    send_blocks(2 * split, fs, True)
+    if split > 1:
+        send_blocks(2, 2 * split)
+    for d in most:
+        steps(3, d, at_end, (True,))
+    send_blocks(2 * split, fs)
 
     def out_copy(k):
         here = pl.ds(pl.multiple_of(k * 2 * model, LANES), 2 * model)
@@ -687,42 +710,26 @@
         out_copy(k).start()
 
     for s in range(STREAMS):
-        cross_line(s).wait_send()
-        if s in BY_COPY:
-            to_copy(s, beyond).wait_send()
-        else:
-            cross_pair(s).wait_send()
-
-        @pl.when(has_left)
-        def _():
-            for side in range(2):
-                on_line(s, 2 * q + side, left_send.at[s, side], left).wait_send()
-
-        @pl.loop(0, fs)
-        def _(source):
-            k = source // 2
-
-            @pl.when(((k <= q) & has_right) | ((k > q) & has_left))
-            def _():
-                on_line(s, source, line_send.at[s, source], across).wait_send()
-
-            @pl.when(k != q)
-            def _():
-                to_copy(s, source).wait_send()
-
-    for copy in (row_to_across, row_to_twin, row_forward, *stat_copies):
-        copy.wait_send()
-
-    @pl.loop(0, fs)
-    def _(b):
-        for side in range(2):
-            last_part(b, side).wait_send()
-        last_copy(b).wait_send()
+        chunks(s, 2, cross_send.at[s]).wait_send()
+        chunks(s, fs - 2, pair_send.at[s]).wait_send()
+    for k in range(lines):
+
+        @pl.when(q == k)
+        def _():
+            for s in range(STREAMS):
+                if k > 0:
+                    chunks(s, 2 * (lines - k), left_send.at[s]).wait_send()
+                if k < lines - 1:
+                    chunks(s, 2 * (k + 1), right_send.at[s]).wait_send()
+
+    bulk(rows_in.at[pl.ds(0, 3)], row_send).wait_send()
+    bulk(stat.at[pl.ds(0, 3)], stat_send).wait_send()
+    bulk(middle.at[:, pl.ds(0, 2)], mid_send).wait_send()
+    bulk(part_out, part_send2).wait_send()
+    bulk(last_in, last_send).wait_send()
 
     @pl.loop(0, lines)
     def _(k):
-        for j in range(2):
-            mid_copy(k, c * 2 + j).wait_send()
         out_copy(k).wait()
 
 
@@ -791,24 +798,25 @@
                 dma((STREAMS + 2,)),
                 dma((lines,)),
                 dma((STREAMS, fs)),
-                dma((STREAMS, fs)),
-                dma((STREAMS, 2)),
-                dma((STREAMS, fs)),
-                dma((STREAMS, fs)),
-                dma((STREAMS, 2)),
-                dma((3,)),
+                dma((2, fs)),
+                dma((STREAMS,)),
+                dma((STREAMS,)),
+                dma((STREAMS,)),
+                dma((STREAMS,)),
+                dma((STREAMS,)),
+                dma(()),
                 dma((4,)),
-                dma((3,)),
+                dma(()),
                 dma((4,)),
+                dma(()),
                 dma((fs,)),
+                dma(()),
                 dma((fs,)),
-                dma((fs,)),
-                dma((fs,)),
-                dma((lines, 4)),
-                dma((lines, 4)),
+                dma(()),
+                dma((4,)),
+                dma(()),
                 dma((fs, 2)),
-                dma((fs, 2)),
-                dma((fs,)),
+                dma(()),
                 dma((fs,)),
             ],
             compiler_params=pltpu.CompilerParams(

time: 158 us -> 151 us (0.956)
  Pallas kernels: 156 us -> 149 us
    pallas_call x1, Pallas kernels: 156 us -> 149 us  [on_device(): pl.pallas_call(functools.partial(kernel, (fs, rows, depth, group, width,...]
where the time goes in v3:
time: 151 us
  Pallas kernels  149 us (99%)
  local copies, waits for them, and re-layouts  2.3 us (2%)
    pallas_call x1, Pallas kernels, on_device(): pl.pallas_call(functools.partial(kernel, (fs, rows, depth, group, width,...  149 us

profile of v3, /device:TPU:0, one launch (start us, length us, event | category | flops | bytes accessed | tf_op | source)
XLA Modules:
  0.0 150.9 jit_solution(12721059279518568224)
XLA Ops:
  0.0 148.6 %shard_map.136 = bf16[256,2048]{1,0:T(8,128)(2,1)} custom-call(bf16[256,2048]{1,0:T(8,128)(2,1)} %residual.1, bf16[256,1024]{1,0:T(8,128)(2,1)} %gating.1, bf16[256,1024]{1,0:T(8,128)(2,1)} %spatial.1, bf16[1024,256]{1,0:T(8,128)(2,1)} %mixer_out.1, bf16[256,1408]{1,0:T(8,128)(2,1)} %gate.1, bf16[256,1408]{1,0:T(8,128)(2,1)} %up.1, bf16[1408,256]{1,0:T(8,128)(2,1)} %down.1, ...), custom_call_target="tpu_custom_call" | custom-call | tf_op jit(solution)/shard_map/pallas_call | solution.py:767
  148.6 2.3 %copy.16 = bf16[256,2048]{1,0:T(8,128)(2,1)} copy(bf16[256,2048]{1,0:T(8,128)(2,1)} %shard_map.136) | data formatting | bytes 2097152

commit v4 on v3

--- a/solution.py
+++ b/solution.py
@@ -222,7 +222,7 @@
     near = jnp.minimum(q, lines - 1 - q)
     at_end, inside = near == 0, near > 0
 
-    def step(s, d, other, who):
+    def from_left(s, d, other, who):
         @pl.when((q - d >= 0) & who)
         def _():
             source = (beyond if other else f) - 2 * d
@@ -234,6 +234,7 @@
 
             to_copy(s, source).start()
 
+    def from_right(s, d, other, who):
         @pl.when((q + d < lines) & who)
         def _():
             source = (beyond if other else f) + 2 * d
@@ -244,6 +245,10 @@
                 on_line(s, source, left_send.at[s], left).start()
 
             to_copy(s, source).start()
+
+    def step(s, d, other, who):
+        from_left(s, d, other, who)
+        from_right(s, d, other, who)
 
     def steps(p, d, who=True, others=(False, True)):
         for other in others:
@@ -552,7 +557,11 @@
 
         @pl.when(i == lines - 1)
         def _():
-            steps(3, 1, inside)
+            for way in (from_right, from_left):
+                for other in (False, True):
+                    for s in PHASES[3]:
+                        way(s, 1, other, inside)
+
             steps(2, last, at_end & (last > 1), (True,))
 
         k = nth(i)
@@ -646,7 +655,6 @@
             give_both(b)
             pass_on(b)
 
-    most = (last,) if last > 1 else ()
     channel(1 - y)
 
     @pl.when(c == 1)
@@ -673,23 +681,35 @@
         pass_on(f)
 
     pass_on(beyond)
+    early = min(4, fs)
+
+    @pl.loop(2, early)
+    def _(i):
+        b = of_block(i)
+        pair_wait(5, b)
+        give(b, 1 - y)
+        pass_on(b)
+
     for d in range(2, last):
         steps(3, d, at_end, (True,))
+    most = (last,) if last > 1 else ()
 
     @pl.loop(0, 2)
     def _(core):
         channel(core * 2 + y)
 
-    for d in most:
-        steps(3, d, at_end, (False,))
-    give(f, y)
-    give(beyond, y)
-    split = lines // 2
-    if split > 1:
-        send_blocks(2, 2 * split)
+        @pl.when(core == 0)
+        def _():
+            for d in most:
+                steps(3, d, at_end, (False,))
+
+    @pl.loop(0, early)
+    def _(i):
+        give(of_block(i), y)
+
     for d in most:
         steps(3, d, at_end, (True,))
-    send_blocks(2 * split, fs)
+    send_blocks(early, fs)
 
     def out_copy(k):
         here = pl.ds(pl.multiple_of(k * 2 * model, LANES), 2 * model)

time: 151 us -> 149 us (0.987)
  Pallas kernels: 149 us -> 147 us
    pallas_call x1, Pallas kernels: 149 us -> 147 us  [on_device(): pl.pallas_call(functools.partial(kernel, (fs, rows, depth, group, width,...]
where the time goes in v4:
time: 149 us
  Pallas kernels  147 us (99%)
  local copies, waits for them, and re-layouts  2.3 us (2%)
    pallas_call x1, Pallas kernels, on_device(): pl.pallas_call(functools.partial(kernel, (fs, rows, depth, group, width,...  147 us

profile of v4, /device:TPU:0, one launch (start us, length us, event | category | flops | bytes accessed | tf_op | source)
XLA Modules:
  0.0 149.1 jit_solution(14532240579909737121)
XLA Ops:
  0.0 146.8 %shard_map.136 = bf16[256,2048]{1,0:T(8,128)(2,1)} custom-call(bf16[256,2048]{1,0:T(8,128)(2,1)} %residual.1, bf16[256,1024]{1,0:T(8,128)(2,1)} %gating.1, bf16[256,1024]{1,0:T(8,128)(2,1)} %spatial.1, bf16[1024,256]{1,0:T(8,128)(2,1)} %mixer_out.1, bf16[256,1408]{1,0:T(8,128)(2,1)} %gate.1, bf16[256,1408]{1,0:T(8,128)(2,1)} %up.1, bf16[1408,256]{1,0:T(8,128)(2,1)} %down.1, ...), custom_call_target="tpu_custom_call" | custom-call | tf_op jit(solution)/shard_map/pallas_call | solution.py:787
  146.8 2.3 %copy.16 = bf16[256,2048]{1,0:T(8,128)(2,1)} copy(bf16[256,2048]{1,0:T(8,128)(2,1)} %shard_map.136) | data formatting | bytes 2097152

commit v5 on v4

--- a/solution.py
+++ b/solution.py
@@ -635,12 +635,6 @@
         part_out[b, side] = dot(hidden[peers + side], g5[b]).astype(BF16)
         last_part(b, side).start()
 
-    def give_both(b):
-        lhs = hidden[pl.ds(peers, 2)].reshape(2 * rows, units)
-        part_out[b] = dot(lhs, g5[b]).reshape(2, rows, model).astype(BF16)
-        for side in range(2):
-            last_part(b, side).start()
-
     def pass_on(b):
         value = dot(hidden[beside], g5[b])
         last_part(b, 1 - y).wait_recv()
@@ -652,7 +646,8 @@
         def _(i):
             b = of_block(i)
             pair_wait(5, b)
-            give_both(b)
+            give(b, 1 - y)
+            give(b, y)
             pass_on(b)
 
     channel(1 - y)

time: 149 us -> 149 us (level)
  no operation moved by 1% of the time
where the time goes in v5:
time: 149 us
  Pallas kernels  147 us (99%)
  local copies, waits for them, and re-layouts  2.3 us (2%)
    pallas_call x1, Pallas kernels, on_device(): pl.pallas_call(functools.partial(kernel, (fs, rows, depth, group, width,...  147 us

profile of v5, /device:TPU:0, one launch (start us, length us, event | category | flops | bytes accessed | tf_op | source)
XLA Modules:
  0.0 148.9 jit_solution(14859670314256973501)
XLA Ops:
  0.0 146.6 %shard_map.136 = bf16[256,2048]{1,0:T(8,128)(2,1)} custom-call(bf16[256,2048]{1,0:T(8,128)(2,1)} %residual.1, bf16[256,1024]{1,0:T(8,128)(2,1)} %gating.1, bf16[256,1024]{1,0:T(8,128)(2,1)} %spatial.1, bf16[1024,256]{1,0:T(8,128)(2,1)} %mixer_out.1, bf16[256,1408]{1,0:T(8,128)(2,1)} %gate.1, bf16[256,1408]{1,0:T(8,128)(2,1)} %up.1, bf16[1408,256]{1,0:T(8,128)(2,1)} %down.1, ...), custom_call_target="tpu_custom_call" | custom-call | tf_op jit(solution)/shard_map/pallas_call | solution.py:782
  146.6 2.3 %copy.16 = bf16[256,2048]{1,0:T(8,128)(2,1)} copy(bf16[256,2048]{1,0:T(8,128)(2,1)} %shard_map.136) | data formatting | bytes 2097152
